TPU v7x, 32 devices: a whole 2x2x4 slice. The times are simulated.
32 devices in a mesh: sp: 16 (over z, y, core), tp: 2 (over x).
Axes of the slice: x: 2, y: 2, z: 4, core: 2. Of those that a mesh axis runs over, the one named last changes fastest.
Arguments:
- stream: bfloat16 [2048, 2048], P('sp', 'tp'), may hold values from -52 to 52
- norm_gain: float32 [2, 2048], replicated, may hold values from 0.1 to 1.9
- value_weight: bfloat16 [4096, 1024], P('sp', 'tp'), may hold values from -0.125 to 0.125
- gate_weight: bfloat16 [4096, 1024], P('sp', 'tp'), may hold values from -0.125 to 0.125
- conv_taps: float32 [2, 31, 1024], replicated, may hold values from -3 to 3
- ln_gain: float32 [2, 1024], replicated, may hold values from 0.1 to 1.9
- ln_bias: float32 [2, 1024], replicated, may hold values from -3 to 3
- out_weight: bfloat16 [1024, 4096], P('tp', 'sp'), may hold values from -0.1875 to 0.1875
- final_gain: float32 [2048], replicated, may hold values from 0.1 to 1.9
Outputs:
- result: bfloat16 [2048, 2048], P('sp', 'tp')
All inputs are finite; a program needn't handle non-finite values.
Results may differ from a plain program's by a relative error of at most 0.014.
Values may be sent and summed in bfloat16 or wider, within the bound.
A program may use at most 64 MiB of HBM per device.

v0:
```python
import jax
import jax.numpy as jnp
from jax import lax
from jax.sharding import PartitionSpec as P

D = 2048
C = 1024
KW = 31
LAYERS = 2
EPS = 1e-06


def from_behind(value, axis, steps):
    count = lax.axis_size(axis)
    first, last = (max(0, -steps), min(count, count - steps))
    return lax.ppermute(value, axis, [(source, source + steps) for source in range(first, last)])


def valid_conv(extended, tap_table):
    length = extended.shape[0] - (KW - 1)
    running = tap_table[0] * extended[0:length]
    for tap_index in range(1, KW):
        running = running + tap_table[tap_index] * extended[tap_index : tap_index + length]
    return running


def local(
    stream,
    norm_gain,
    value_weight,
    gate_weight,
    conv_taps,
    ln_gain,
    ln_bias,
    out_weight,
    final_gain,
):
    tokens_here = stream.shape[0]
    columns = stream.shape[1]
    channels = value_weight.shape[1]
    rim_rows = KW - 1
    tp_index = lax.axis_index("tp")
    my_taps = lax.dynamic_slice_in_dim(conv_taps, tp_index * channels, channels, 2)
    my_ln_gain = lax.dynamic_slice_in_dim(ln_gain, tp_index * channels, channels, 1)
    my_ln_bias = lax.dynamic_slice_in_dim(ln_bias, tp_index * channels, channels, 1)
    my_final = lax.dynamic_slice_in_dim(final_gain, tp_index * columns, columns, 0)
    value_all, gate_all, out_all = (
        lax.all_gather(value_weight, "sp", axis=0, tiled=True),
        lax.all_gather(gate_weight, "sp", axis=0, tiled=True),
        lax.all_gather(out_weight, "sp", axis=1, tiled=True),
    )
    value_all = value_all.reshape(D, LAYERS, channels)
    gate_all = gate_all.reshape(D, LAYERS, channels)
    out_all = out_all.reshape(channels, D, LAYERS)
    earlier = from_behind(stream[-LAYERS * rim_rows :], "sp", 1)
    current = jnp.concatenate([earlier, stream], axis=0)
    for layer_index in range(LAYERS):
        prefix = (LAYERS - layer_index) * rim_rows
        gathered = lax.all_gather(current, "tp", axis=1, tiled=True)
        gathered32 = gathered.astype(jnp.float32)
        scale = lax.rsqrt(jnp.sum(gathered32 * gathered32, axis=1, keepdims=True) / D + EPS)
        run_normed = (gathered32 * scale * norm_gain[layer_index]).astype(jnp.bfloat16)
        value_proj = jnp.dot(
            run_normed, value_all[:, layer_index], preferred_element_type=jnp.float32
        )
        gate_proj = jnp.dot(
            run_normed, gate_all[:, layer_index], preferred_element_type=jnp.float32
        )
        glu_out = value_proj * jax.nn.sigmoid(gate_proj)
        positions = (
            lax.axis_index("sp") * tokens_here - prefix + lax.iota(jnp.int32, current.shape[0])
        )
        extended = jnp.where((positions >= 0)[:, None], glu_out, 0.0)
        residual = current[rim_rows:].astype(jnp.float32)
        conv_out = valid_conv(extended, my_taps[layer_index])
        first_sums, square_sums = lax.psum(
            (jnp.sum(conv_out, axis=1), jnp.sum(conv_out * conv_out, axis=1)), "tp"
        )
        row_mean = (first_sums / C)[:, None]
        row_var = (square_sums / C)[:, None] - row_mean * row_mean
        run_active = jax.nn.silu(
            (conv_out - row_mean) * lax.rsqrt(row_var + EPS) * my_ln_gain[layer_index]
            + my_ln_bias[layer_index]
        ).astype(jnp.bfloat16)
        partial_value = jnp.dot(
            run_active, out_all[:, :, layer_index], preferred_element_type=jnp.float32
        )
        summed = lax.psum_scatter(
            partial_value.astype(jnp.bfloat16), "tp", scatter_dimension=1, tiled=True
        ).astype(jnp.float32)
        current = (residual + summed).astype(jnp.bfloat16)
    final32 = current.astype(jnp.float32)
    squares = lax.psum(jnp.sum(final32 * final32, axis=1), "tp")
    return (final32 * lax.rsqrt(squares[:, None] / D + EPS) * my_final).astype(jnp.bfloat16)


def solution(mesh):
    placed = (P("sp", "tp"), P(), P("sp", "tp"), P("sp", "tp"), P(), P(), P(), P("tp", "sp"), P())
    return jax.shard_map(
        local, mesh=mesh, in_specs=placed, out_specs=P("sp", "tp"), check_vma=False
    )
```

profile of v0, /device:TPU:0, one launch (start us, length us, event | category | flops | bytes accessed | tf_op | source)
XLA Modules:
  0.0 278.0 jit_solution(3715247902081535697)
XLA Ops:
  6.5 0.7 all-gather.6.cloned.1.call-update
  7.3 0.0 all-gather.4.cloned.1.call-start
  7.3 0.7 all-gather.4.cloned.1.call-update
  8.0 0.0 all-gather.8.cloned.1.call-start
  8.1 0.7 all-gather.8.cloned.1.call-update
  8.7 0.0 reduce-scatter.3.cloned.1.call-start
  8.8 0.9 slice.543
  9.7 2.4 collective-permute-start
  12.2 0.8 fusion.145
  13.0 1.0 fusion.143
  14.0 0.8 fusion.144
  14.9 1.3 constant_dynamic-slice_fusion.33
  16.2 1.0 pad_maximum_fusion
  17.2 11.7 %all_gather.15 = bf16[188,2048]{1,0:T(8,128)(2,1)S(1)} all-gather(bf16[188,1024]{1,0:T(8,128)(2,1)S(1)} %pad_maximum_fusion), channel_id=1, replica_groups=mesh['sp'=16,'tp'=2] {'tp'}, dimensions={1}, use_global_device_ids=true | all-gather | bytes 1155072 | tf_op jit(solution)/shard_map/all_gather | solution.py:59
  28.9 0.2 fusion.14
  29.1 33.5 %all-gather.6.cloned.1.call-done = bf16[4096,512]{1,0:T(8,128)(2,1)} async-done(((bf16[256,512]{1,0:T(8,128)(2,1)}), bf16[4096,512]{1,0:T(8,128)(2,1)}) %all-gather.6.cloned.1.call-update) | async-done | bytes 4194320 | tf_op jit(solution)/shard_map/all_gather | solution.py:49
  62.6 7.2 %reshape.177 = bf16[2048,2,512]{2,1,0:T(2,128)(2,1)} reshape(bf16[4096,512]{1,0:T(8,128)(2,1)} %all-gather.6.cloned.1.call-done) | data formatting | bytes 8388608 | tf_op jit(solution)/shard_map/reshape | solution.py:53
  69.8 43.9 %all-gather.4.cloned.1.call-done = bf16[4096,512]{1,0:T(8,128)(2,1)} async-done(((bf16[256,512]{1,0:T(8,128)(2,1)}), bf16[4096,512]{1,0:T(8,128)(2,1)}) %all-gather.4.cloned.1.call-update) | async-done | bytes 4194320 | tf_op jit(solution)/shard_map/all_gather | solution.py:48
  113.7 7.2 %reshape.176 = bf16[2048,2,512]{2,1,0:T(2,128)(2,1)} reshape(bf16[4096,512]{1,0:T(8,128)(2,1)} %all-gather.4.cloned.1.call-done) | data formatting | bytes 8388608 | tf_op jit(solution)/shard_map/reshape | solution.py:52
  120.9 10.0 %fusion.141 = (bf16[2048,1,512]{2,1,0:T(2,128)(2,1)}, bf16[2048,1,512]{2,1,0:T(2,128)(2,1)}) fusion(bf16[2048,2,512]{2,1,0:T(2,128)(2,1)} %reshape.177), kind=kLoop, calls=%fused_computation.233 | loop fusion | bytes 8388608 | tf_op jit(solution)/shard_map/slice | solution.py:67
  130.9 7.0 %fusion.140 = (bf16[2048,1,512]{2,1,0:T(2,128)(2,1)}, bf16[2048,1,512]{2,1,0:T(2,128)(2,1)}) fusion(bf16[2048,2,512]{2,1,0:T(2,128)(2,1)S(1)} %copy-done), kind=kLoop, calls=%fused_computation.232 | loop fusion | bytes 8388608 | tf_op jit(solution)/shard_map/slice | solution.py:64
  137.9 29.0 %all-gather.8.cloned.1.call-done = bf16[512,4096]{1,0:T(8,128)(2,1)} async-done(((bf16[512,256]{1,0:T(8,128)(2,1)}), bf16[512,4096]{1,0:T(8,128)(2,1)}) %all-gather.8.cloned.1.call-update) | async-done | bytes 4194320 | tf_op jit(solution)/shard_map/all_gather | solution.py:50
  166.9 6.5 %copy.13 = bf16[512,4096]{0,1:T(8,128)(2,1)} copy(bf16[512,4096]{1,0:T(8,128)(2,1)} %all-gather.8.cloned.1.call-done) | data formatting | bytes 8388608 | tf_op jit(solution)/shard_map/all_gather | solution.py:50
  173.4 7.2 %reshape.178 = bf16[512,2048,2]{0,2,1:T(2,128)(2,1)} reshape(bf16[512,4096]{0,1:T(8,128)(2,1)} %copy.13) | data formatting | bytes 8388608 | tf_op jit(solution)/shard_map/reshape | solution.py:54
  180.6 9.9 %fusion.142 = (bf16[512,2048,1]{0,2,1:T(2,128)(2,1)}, bf16[512,2048,1]{0,2,1:T(2,128)(2,1)}) fusion(bf16[512,2048,2]{0,2,1:T(2,128)(2,1)} %reshape.178), kind=kLoop, calls=%fused_computation.234 | loop fusion | bytes 8388608 | tf_op jit(solution)/shard_map/slice | solution.py:86
  190.5 9.0 %copy.14 = bf16[512,2048,1]{1,0,2:T(8,128)(2,1)S(1)} copy(bf16[512,2048,1]{0,2,1:T(2,128)(2,1)} %get-tuple-element.19) | data formatting | bytes 4194304 | tf_op jit(solution)/shard_map/slice | solution.py:86
  199.5 3.0 %fusion.29 = f32[188,512]{1,0:T(8,128)S(1)} fusion(bf16[2048,1,512]{2,1,0:T(2,128)(2,1)} %get-tuple-element.17, bf16[188,2048]{1,0:T(8,128)(2,1)S(1)} %all_gather.15, f32[2048]{0:T(1024)S(1)} %bitcast.145, f32[188]{0:T(256)S(1)} %add_rsqrt_fusion.2), kind=kOutput, calls=%fused_computation.29 | convolution fusion | flops 396093440 | bytes 3261168 | tf_op jit(solution)/shard_map/dot_general | solution.py:66
  202.6 0.4 copy-done.2
  203.0 0.6 fusion.35
  203.6 1.5 fusion.136
  205.1 4.9 %all-reduce.1 = (f32[158]{0:T(256)S(1)}, f32[158]{0:T(256)S(1)}) all-reduce(f32[158]{0:T(256)S(1)} %get-tuple-element.6, f32[158]{0:T(256)S(1)} %get-tuple-element.5), channel_id=1, replica_groups=mesh['sp'=16,'tp'=2] {'tp'}, use_global_device_ids=true, to_apply=%region_4.5 | all-reduce | flops 316 | bytes 2528 | tf_op jit(solution)/shard_map/psum | solution.py:76
  210.0 1.5 convolution_convert_fusion
  211.6 0.0 reduce-scatter.5.cloned.1.call-start
  211.7 9.1 %copy.15 = bf16[512,2048,1]{1,0,2:T(8,128)(2,1)S(1)} copy(bf16[512,2048,1]{0,2,1:T(2,128)(2,1)} %get-tuple-element.20) | data formatting | bytes 4194304 | tf_op jit(solution)/shard_map/slice | solution.py:86
  220.7 5.3 %reduce-scatter.3.cloned.1.call-done = bf16[158,1024]{1,0:T(8,128)(2,1)} async-done(((bf16[158,2048]{1,0:T(8,128)(2,1)}), bf16[158,1024]{1,0:T(8,128)(2,1)}) %reduce-scatter.3.cloned.1.call-update) | async-done | bytes 323600 | tf_op jit(solution)/shard_map/reduce_scatter | solution.py:88
  226.0 1.1 add_convert_fusion
  227.1 9.9 %all_gather.19 = bf16[158,2048]{1,0:T(8,128)(2,1)S(1)} all-gather(bf16[158,1024]{1,0:T(8,128)(2,1)S(1)} %add_convert_fusion), channel_id=1, replica_groups=mesh['sp'=16,'tp'=2] {'tp'}, dimensions={1}, use_global_device_ids=true | all-gather | bytes 970752 | tf_op jit(solution)/shard_map/all_gather | solution.py:59
  237.0 0.2 fusion.17
  237.3 3.0 %fusion.50 = f32[158,512]{1,0:T(8,128)S(1)} fusion(bf16[2048,1,512]{2,1,0:T(2,128)(2,1)} %get-tuple-element.18, bf16[158,2048]{1,0:T(8,128)(2,1)S(1)} %all_gather.19, f32[2048]{0:T(1024)S(1)} %bitcast.143, f32[158]{0:T(256)S(1)} %add_rsqrt_fusion), kind=kOutput, calls=%fused_computation.36 | convolution fusion | flops 332887040 | bytes 3076728 | tf_op jit(solution)/shard_map/dot_general | solution.py:66
  240.2 0.5 copy-done.1
  240.7 0.6 fusion.53
  241.3 1.1 fusion.137
  242.4 4.9 %all-reduce = (f32[128]{0:T(128)S(1)}, f32[128]{0:T(128)S(1)}) all-reduce(f32[128]{0:T(128)S(1)} %get-tuple-element.8, f32[128]{0:T(128)S(1)} %get-tuple-element.7), channel_id=1, replica_groups=mesh['sp'=16,'tp'=2] {'tp'}, use_global_device_ids=true, to_apply=%region_10.11 | all-reduce | flops 256 | bytes 2048 | tf_op jit(solution)/shard_map/psum | solution.py:76
  247.4 1.3 convolution_convert_fusion.1
  248.8 14.8 %reduce-scatter.5.cloned.1.call-done = bf16[128,1024]{1,0:T(8,128)(2,1)} async-done(((bf16[128,2048]{1,0:T(8,128)(2,1)}), bf16[128,1024]{1,0:T(8,128)(2,1)}) %reduce-scatter.5.cloned.1.call-update) | async-done | bytes 262160 | tf_op jit(solution)/shard_map/reduce_scatter | solution.py:88
  263.6 1.2 fusion.56
  264.7 4.9 %psum.39 = f32[128]{0:T(128)S(1)} all-reduce(f32[128]{0:T(128)S(1)} %fusion.56), channel_id=1, replica_groups=mesh['sp'=16,'tp'=2] {'tp'}, use_global_device_ids=true, to_apply=%region_13.14 | all-reduce | flops 128 | bytes 1024 | tf_op jit(solution)/shard_map/psum | solution.py:93
  269.6 1.8 fusion.58
  (20 shorter events, 0.1 us)
Async XLA Ops:
  6.5 56.1 %all-gather.6.cloned.1.call-start = ((), (), s32[]{:S(2)}) async-start(), calls=%async_computation.3 | async-start | bytes 4456448 | tf_op jit(solution)/shard_map/all_gather | solution.py:49
  7.3 106.5 %all-gather.4.cloned.1.call-start = ((), (), s32[]{:S(2)}) async-start(), calls=%async_computation.2 | async-start | bytes 4456448 | tf_op jit(solution)/shard_map/all_gather | solution.py:48
  8.0 158.9 %all-gather.8.cloned.1.call-start = ((), (), s32[]{:S(2)}) async-start(), calls=%async_computation.4 | async-start | bytes 4456448 | tf_op jit(solution)/shard_map/all_gather | solution.py:50
  8.7 217.3 %reduce-scatter.3.cloned.1.call-start = ((), (), s32[]{:S(2)}) async-start(), calls=%async_computation.5 | async-start | bytes 983040 | tf_op jit(solution)/shard_map/reduce_scatter | solution.py:88
  9.7 6.4 %collective-permute-start = (bf16[60,1024]{1,0:T(8,128)(2,1)S(1)}, bf16[60,1024]{1,0:T(8,128)(2,1)S(1)}, u32[]{:S(2)}, u32[]{:S(2)}) collective-permute-start(bf16[60,1024]{1,0:T(8,128)(2,1)S(1)} %slice.543), channel_id=1, source_target_pairs={{0,2},{2,4},{4,6},{6,8},{8,10},{10,12},{12,14},{14,16},{16,18},{18... | collective-permute-start | bytes 368648 | tf_op jit(solution)/shard_map/ppermute | solution.py:16
  120.9 10.0 %copy-start = (bf16[2048,2,512]{2,1,0:T(2,128)(2,1)S(1)}, bf16[2048,2,512]{2,1,0:T(2,128)(2,1)}, u32[]{:S(2)}) copy-start(bf16[2048,2,512]{2,1,0:T(2,128)(2,1)} %reshape.176) | copy-start | bytes 12582916
  199.5 3.5 %copy-start.2 = (bf16[2048,1,512]{2,1,0:T(2,128)(2,1)S(1)}, bf16[2048,1,512]{2,1,0:T(2,128)(2,1)}, u32[]{:S(2)}) copy-start(bf16[2048,1,512]{2,1,0:T(2,128)(2,1)} %get-tuple-element.16) | copy-start | bytes 6291460
  211.6 52.0 %reduce-scatter.5.cloned.1.call-start = ((), (), s32[]{:S(2)}) async-start(), calls=%async_computation.6 | async-start | bytes 786432 | tf_op jit(solution)/shard_map/reduce_scatter | solution.py:88
  211.7 14.3 %copy-start.3 = (bf16[128,1024]{1,0:T(8,128)(2,1)S(1)}, bf16[128,1024]{1,0:T(8,128)(2,1)}, u32[]{:S(2)}) copy-start(bf16[128,1024]{1,0:T(8,128)(2,1)} %param.9) | copy-start | bytes 786436
  237.2 3.5 %copy-start.1 = (bf16[2048,1,512]{2,1,0:T(2,128)(2,1)S(1)}, bf16[2048,1,512]{2,1,0:T(2,128)(2,1)}, u32[]{:S(2)}) copy-start(bf16[2048,1,512]{2,1,0:T(2,128)(2,1)} %get-tuple-element.15) | copy-start | bytes 6291460
  242.4 6.3 %copy-start.4 = (f32[2048]{0:T(1024)S(1)}, f32[2048]{0:T(1024)}, u32[]{:S(2)}) copy-start(f32[2048]{0:T(1024)} %param.17) | copy-start | bytes 24580
Sparse Core Ops, SparseCore 0:
  9.5 53.0 all-gather.5
  64.8 48.8 all-gather.3
  115.9 50.9 all-gather.7
  211.7 14.2 reduce-scatter.2
  248.8 14.6 reduce-scatter.4
where the time goes:
time: 279 us; the launch traced here: 278 us
  waiting for transfers between devices  129 us (46%)
  local copies, waits for them, and re-layouts  78.9 us (28%)
  blocking collectives  36.4 us (13%)
  between operations  13.3 us (5%)
  matrix products  10 us (4%)
  other arithmetic  8.25 us (3%)
    all_gather x1, waiting for transfers between devices, local(): lax.all_gather(value_weight, 'sp', axis=0, tiled=True)  43.9 us
    all_gather x1, waiting for transfers between devices, local(): lax.all_gather(gate_weight, 'sp', axis=0, tiled=True)  33.5 us
    all_gather x1, waiting for transfers between devices, local(): lax.all_gather(out_weight, 'sp', axis=1, tiled=True)  29 us
    slice x3, local copies, waits for them, and re-layouts, local(): out_all[:, :, layer_index]  28 us
    all_gather x2, blocking collectives, local(): gathered = lax.all_gather(current, 'tp', axis=1, tiled=True)  21.6 us
    reduce_scatter x2, waiting for transfers between devices, local(): lax.psum_scatter(partial_value.astype(jnp.bfloat16), 'tp', scatter_dimens...  20.1 us
    slice x1, local copies, waits for them, and re-layouts, local(): gate_all[:, layer_index]  9.98 us
    psum x2, blocking collectives, local(): lax.psum((jnp.sum(conv_out, axis=1), jnp.sum(conv_out * conv_out, axis=1)...  9.87 us
  transfers between devices with their start and end apart: 6, of which 5 were waited for; matrix products, arithmetic and copies ran while one was open for 17% of the time, Pallas kernels for 0%

commit v1 on v0

--- a/solution.py
+++ b/solution.py
@@ -56,7 +56,8 @@
     current = jnp.concatenate([earlier, stream], axis=0)
     for layer_index in range(LAYERS):
         prefix = (LAYERS - layer_index) * rim_rows
-        gathered = lax.all_gather(current, "tp", axis=1, tiled=True)
+        shards = lax.all_gather(current, "tp")
+        gathered = jnp.concatenate(shards, axis=1)
         gathered32 = gathered.astype(jnp.float32)
         scale = lax.rsqrt(jnp.sum(gathered32 * gathered32, axis=1, keepdims=True) / D + EPS)
         run_normed = (gathered32 * scale * norm_gain[layer_index]).astype(jnp.bfloat16)

time: 279 us -> 281 us (level)
  local copies, waits for them, and re-layouts: 78.9 us -> 83.5 us
    unnamed x10 -> x16, local copies, waits for them, and re-layouts: 0.92 us -> 4.16 us
where the time goes in v1:
time: 281 us; the launch traced here: 279 us
  waiting for transfers between devices  127 us (45%)
  local copies, waits for them, and re-layouts  83.5 us (30%)
  blocking collectives  36.6 us (13%)
  between operations  13.4 us (5%)
  other arithmetic  8.73 us (3%)
  matrix products  7.5 us (3%)
    all_gather x1, waiting for transfers between devices, local(): lax.all_gather(value_weight, 'sp', axis=0, tiled=True)  43.9 us
    all_gather x1, waiting for transfers between devices, local(): lax.all_gather(gate_weight, 'sp', axis=0, tiled=True)  31.6 us
    all_gather x1, waiting for transfers between devices, local(): lax.all_gather(out_weight, 'sp', axis=1, tiled=True)  29.2 us
    slice x3, local copies, waits for them, and re-layouts, local(): out_all[:, :, layer_index]  28 us
    all_gather x2, blocking collectives, local(): shards = lax.all_gather(current, 'tp')  21.8 us
    reduce_scatter x2, waiting for transfers between devices, local(): lax.psum_scatter(partial_value.astype(jnp.bfloat16), 'tp', scatter_dimens...  20 us
    psum x2, blocking collectives, local(): lax.psum((jnp.sum(conv_out, axis=1), jnp.sum(conv_out * conv_out, axis=1)...  9.87 us
    slice x1, local copies, waits for them, and re-layouts, local(): gate_all[:, layer_index]  9.81 us
  transfers between devices with their start and end apart: 6, of which 5 were waited for; matrix products, arithmetic and copies ran while one was open for 17% of the time, Pallas kernels for 0%

profile of v1, /device:TPU:0, one launch (start us, length us, event | category | flops | bytes accessed | tf_op | source)
XLA Modules:
  0.0 279.0 jit_solution(6128244267186683800)
XLA Ops:
  6.5 0.7 all-gather.10.cloned.1.call-update
  7.3 0.7 all-gather.8.cloned.1.call-update
  8.1 0.7 all-gather.12.cloned.1.call-update
  8.8 0.9 slice.543
  9.7 2.4 collective-permute-start
  12.2 0.8 fusion.143
  13.0 1.0 fusion.142
  14.0 0.8 slice_reduce_fusion
  14.9 1.3 constant_dynamic-slice_fusion.33
  16.2 1.0 fusion.61
  17.2 11.7 %all-gather.2 = bf16[2,188,1024]{2,1,0:T(8,128)(2,1)S(1)} all-gather(bf16[1,188,1024]{2,1,0:T(8,128)(2,1)S(1)} %fusion.61), channel_id=2, replica_groups=mesh['sp'=16,'tp'=2] {'tp'}, dimensions={0}, use_global_device_ids=true | all-gather | bytes 1155072 | tf_op jit(solution)/shard_map/all_gather | solution.py:59
  29.1 0.3 fusion.56
  29.4 0.8 copy.20
  30.2 0.6 pad.2
  31.0 31.6 %all-gather.10.cloned.1.call-done = bf16[4096,512]{1,0:T(8,128)(2,1)} async-done(((bf16[256,512]{1,0:T(8,128)(2,1)}), bf16[4096,512]{1,0:T(8,128)(2,1)}) %all-gather.10.cloned.1.call-update) | async-done | bytes 4194320 | tf_op jit(solution)/shard_map/all_gather | solution.py:49
  62.6 7.2 %reshape.225 = bf16[2048,2,512]{2,1,0:T(2,128)(2,1)} reshape(bf16[4096,512]{1,0:T(8,128)(2,1)} %all-gather.10.cloned.1.call-done) | data formatting | bytes 8388608 | tf_op jit(solution)/shard_map/reshape | solution.py:53
  69.8 43.9 %all-gather.8.cloned.1.call-done = bf16[4096,512]{1,0:T(8,128)(2,1)} async-done(((bf16[256,512]{1,0:T(8,128)(2,1)}), bf16[4096,512]{1,0:T(8,128)(2,1)}) %all-gather.8.cloned.1.call-update) | async-done | bytes 4194320 | tf_op jit(solution)/shard_map/all_gather | solution.py:48
  113.7 7.2 %reshape.224 = bf16[2048,2,512]{2,1,0:T(2,128)(2,1)} reshape(bf16[4096,512]{1,0:T(8,128)(2,1)} %all-gather.8.cloned.1.call-done) | data formatting | bytes 8388608 | tf_op jit(solution)/shard_map/reshape | solution.py:52
  120.9 9.8 %fusion.140 = (bf16[2048,1,512]{2,1,0:T(2,128)(2,1)}, bf16[2048,1,512]{2,1,0:T(2,128)(2,1)}) fusion(bf16[2048,2,512]{2,1,0:T(2,128)(2,1)} %reshape.225), kind=kLoop, calls=%fused_computation.238 | loop fusion | bytes 8388608 | tf_op jit(solution)/shard_map/slice | solution.py:68
  130.8 7.0 %fusion.139 = (bf16[2048,1,512]{2,1,0:T(2,128)(2,1)}, bf16[2048,1,512]{2,1,0:T(2,128)(2,1)}) fusion(bf16[2048,2,512]{2,1,0:T(2,128)(2,1)S(1)} %copy-done), kind=kLoop, calls=%fused_computation.237 | loop fusion | bytes 8388608 | tf_op jit(solution)/shard_map/slice | solution.py:65
  137.8 29.2 %all-gather.12.cloned.1.call-done = bf16[512,4096]{1,0:T(8,128)(2,1)} async-done(((bf16[512,256]{1,0:T(8,128)(2,1)}), bf16[512,4096]{1,0:T(8,128)(2,1)}) %all-gather.12.cloned.1.call-update) | async-done | bytes 4194320 | tf_op jit(solution)/shard_map/all_gather | solution.py:50
  166.9 6.5 %copy.21 = bf16[512,4096]{0,1:T(8,128)(2,1)} copy(bf16[512,4096]{1,0:T(8,128)(2,1)} %all-gather.12.cloned.1.call-done) | data formatting | bytes 8388608 | tf_op jit(solution)/shard_map/all_gather | solution.py:50
  173.4 7.2 %reshape.226 = bf16[512,2048,2]{0,2,1:T(2,128)(2,1)} reshape(bf16[512,4096]{0,1:T(8,128)(2,1)} %copy.21) | data formatting | bytes 8388608 | tf_op jit(solution)/shard_map/reshape | solution.py:54
  180.6 9.9 %fusion.141 = (bf16[512,2048,1]{0,2,1:T(2,128)(2,1)}, bf16[512,2048,1]{0,2,1:T(2,128)(2,1)}) fusion(bf16[512,2048,2]{0,2,1:T(2,128)(2,1)} %reshape.226), kind=kLoop, calls=%fused_computation.239 | loop fusion | bytes 8388608 | tf_op jit(solution)/shard_map/slice | solution.py:87
  190.5 9.0 %copy.22 = bf16[512,2048,1]{1,0,2:T(8,128)(2,1)S(1)} copy(bf16[512,2048,1]{0,2,1:T(2,128)(2,1)} %get-tuple-element.21) | data formatting | bytes 4194304 | tf_op jit(solution)/shard_map/slice | solution.py:87
  199.5 3.0 %fusion.29 = f32[188,512]{1,0:T(8,128)S(1)} fusion(bf16[188,2048]{1,0:T(8,128)(2,1)S(1)} %bitcast.130, bf16[2048,1,512]{2,1,0:T(2,128)(2,1)} %get-tuple-element.20), kind=kOutput, calls=%fused_computation.29 | convolution fusion | flops 394553344 | bytes 3252224 | tf_op jit(solution)/shard_map/dot_general | solution.py:67
  202.5 0.5 copy-done.3
  203.0 0.6 fusion.35
  203.6 1.5 fusion.135
  205.1 4.9 %all-reduce.1 = (f32[158]{0:T(256)S(1)}, f32[158]{0:T(256)S(1)}) all-reduce(f32[158]{0:T(256)S(1)} %get-tuple-element.6, f32[158]{0:T(256)S(1)} %get-tuple-element.5), channel_id=1, replica_groups=mesh['sp'=16,'tp'=2] {'tp'}, use_global_device_ids=true, to_apply=%region_4.5 | all-reduce | flops 316 | bytes 2528 | tf_op jit(solution)/shard_map/psum | solution.py:77
  210.0 1.5 convolution_convert_fusion
  211.7 9.1 %copy.24 = bf16[512,2048,1]{1,0,2:T(8,128)(2,1)S(1)} copy(bf16[512,2048,1]{0,2,1:T(2,128)(2,1)} %get-tuple-element.22) | data formatting | bytes 4194304 | tf_op jit(solution)/shard_map/slice | solution.py:87
  220.7 5.2 %reduce-scatter.3.cloned.1.call-done = bf16[158,1024]{1,0:T(8,128)(2,1)} async-done(((bf16[158,2048]{1,0:T(8,128)(2,1)}), bf16[158,1024]{1,0:T(8,128)(2,1)}) %reduce-scatter.3.cloned.1.call-update) | async-done | bytes 323600 | tf_op jit(solution)/shard_map/reduce_scatter | solution.py:89
  226.0 1.1 add_convert_fusion
  227.1 10.1 %all-gather.3 = bf16[2,158,1024]{2,1,0:T(8,128)(2,1)S(1)} all-gather(bf16[1,158,1024]{2,1,0:T(8,128)(2,1)S(1)} %bitcast.127), channel_id=3, replica_groups=mesh['sp'=16,'tp'=2] {'tp'}, dimensions={0}, use_global_device_ids=true | all-gather | bytes 970752 | tf_op jit(solution)/shard_map/all_gather | solution.py:59
  237.7 0.7 copy.23
  238.3 0.5 pad.3
  239.0 0.6 copy-done.1
  239.6 0.6 fusion.50
  240.2 1.6 copy-done.2
  241.8 0.5 fusion.53
  242.3 1.1 fusion.136
  243.5 4.9 %all-reduce = (f32[128]{0:T(128)S(1)}, f32[128]{0:T(128)S(1)}) all-reduce(f32[128]{0:T(128)S(1)} %get-tuple-element.8, f32[128]{0:T(128)S(1)} %get-tuple-element.7), channel_id=1, replica_groups=mesh['sp'=16,'tp'=2] {'tp'}, use_global_device_ids=true, to_apply=%region_10.11 | all-reduce | flops 256 | bytes 2048 | tf_op jit(solution)/shard_map/psum | solution.py:77
  248.4 1.4 convolution_convert_fusion.1
  249.8 14.8 %reduce-scatter.5.cloned.1.call-done = bf16[128,1024]{1,0:T(8,128)(2,1)} async-done(((bf16[128,2048]{1,0:T(8,128)(2,1)}), bf16[128,1024]{1,0:T(8,128)(2,1)}) %reduce-scatter.5.cloned.1.call-update) | async-done | bytes 262160 | tf_op jit(solution)/shard_map/reduce_scatter | solution.py:89
  264.6 1.2 fusion.58
  265.8 4.9 %psum.39 = f32[128]{0:T(128)S(1)} all-reduce(f32[128]{0:T(128)S(1)} %fusion.58), channel_id=1, replica_groups=mesh['sp'=16,'tp'=2] {'tp'}, use_global_device_ids=true, to_apply=%region_13.14 | all-reduce | flops 128 | bytes 1024 | tf_op jit(solution)/shard_map/psum | solution.py:94
  270.7 1.8 fusion.60
  (32 shorter events, 1.3 us)
Async XLA Ops:
  6.5 56.1 %all-gather.10.cloned.1.call-start = ((), (), s32[]{:S(2)}) async-start(), calls=%async_computation.3 | async-start | bytes 4456448 | tf_op jit(solution)/shard_map/all_gather | solution.py:49
  7.3 106.5 %all-gather.8.cloned.1.call-start = ((), (), s32[]{:S(2)}) async-start(), calls=%async_computation.2 | async-start | bytes 4456448 | tf_op jit(solution)/shard_map/all_gather | solution.py:48
  8.0 158.9 %all-gather.12.cloned.1.call-start = ((), (), s32[]{:S(2)}) async-start(), calls=%async_computation.4 | async-start | bytes 4456448 | tf_op jit(solution)/shard_map/all_gather | solution.py:50
  8.7 217.2 %reduce-scatter.3.cloned.1.call-start = ((), (), s32[]{:S(2)}) async-start(), calls=%async_computation.5 | async-start | bytes 983040 | tf_op jit(solution)/shard_map/reduce_scatter | solution.py:89
  9.7 6.5 %collective-permute-start = (bf16[60,1024]{1,0:T(8,128)(2,1)S(1)}, bf16[60,1024]{1,0:T(8,128)(2,1)S(1)}, u32[]{:S(2)}, u32[]{:S(2)}) collective-permute-start(bf16[60,1024]{1,0:T(8,128)(2,1)S(1)} %slice.543), channel_id=1, source_target_pairs={{0,2},{2,4},{4,6},{6,8},{8,10},{10,12},{12,14},{14,16},{16,18},{18... | collective-permute-start | bytes 368648 | tf_op jit(solution)/shard_map/ppermute | solution.py:16
  120.9 9.8 %copy-start = (bf16[2048,2,512]{2,1,0:T(2,128)(2,1)S(1)}, bf16[2048,2,512]{2,1,0:T(2,128)(2,1)}, u32[]{:S(2)}) copy-start(bf16[2048,2,512]{2,1,0:T(2,128)(2,1)} %reshape.224) | copy-start | bytes 12582916
  199.5 3.5 %copy-start.3 = (bf16[2048,1,512]{2,1,0:T(2,128)(2,1)S(1)}, bf16[2048,1,512]{2,1,0:T(2,128)(2,1)}, u32[]{:S(2)}) copy-start(bf16[2048,1,512]{2,1,0:T(2,128)(2,1)} %get-tuple-element.18) | copy-start | bytes 6291460
  211.6 53.0 %reduce-scatter.5.cloned.1.call-start = ((), (), s32[]{:S(2)}) async-start(), calls=%async_computation.6 | async-start | bytes 786432 | tf_op jit(solution)/shard_map/reduce_scatter | solution.py:89
  211.6 14.3 %copy-start.4 = (bf16[128,1024]{1,0:T(8,128)(2,1)S(1)}, bf16[128,1024]{1,0:T(8,128)(2,1)}, u32[]{:S(2)}) copy-start(bf16[128,1024]{1,0:T(8,128)(2,1)} %param.9) | copy-start | bytes 786436
  237.4 2.2 copy-start.1
  239.6 2.2 copy-start.2
  243.5 6.3 %copy-start.5 = (f32[2048]{0:T(1024)S(1)}, f32[2048]{0:T(1024)}, u32[]{:S(2)}) copy-start(f32[2048]{0:T(1024)} %param.17) | copy-start | bytes 24580
Sparse Core Ops, SparseCore 0:
  9.5 53.0 all-gather.9
  64.8 48.8 all-gather.7
  115.9 50.9 all-gather.11
  211.7 14.2 reduce-scatter.2
  249.9 14.6 reduce-scatter.4
